TPU v7x, 32 devices: a whole 2x2x4 slice. The times are simulated.
32 devices in a mesh: fs: 16 (over z, y, x), tp: 2 (over core).
Axes of the slice: x: 2, y: 2, z: 4, core: 2. Of those that a mesh axis runs over, the one named last changes fastest.
Arguments:
- tokens: bfloat16 [4096, 2048], P('fs'), may hold values from -6 to 6
- routes: int32 [4096, 6], P('fs'), may hold values from 0 to 15, all different within a row; in each aligned block of 256 rows (0 to 255, 256 to 511, ...) at most 160 rows name the same one
- route_weights: float32 [4096, 6], P('fs'), may hold values from 0.1 to 1
- norm_gain: float32 [2048], P('fs'), may hold values from 0.1 to 1.9
- expert_gate: float32 [16, 2048, 1024], P(None, 'fs', 'tp'), may hold values from -0.125 to 0.125
- expert_up: float32 [16, 2048, 1024], P(None, 'fs', 'tp'), may hold values from -0.125 to 0.125
- expert_down: float32 [16, 2048, 1024], P(None, 'fs', 'tp'), may hold values from -0.1875 to 0.1875
- shared_gate: float32 [2048, 1024], P('fs', 'tp'), may hold values from -0.125 to 0.125
- shared_up: float32 [2048, 1024], P('fs', 'tp'), may hold values from -0.125 to 0.125
- shared_down: float32 [2048, 1024], P('fs', 'tp'), may hold values from -0.1875 to 0.1875
Outputs:
- layer_output: bfloat16 [4096, 2048], P('fs', 'tp')
- sample_gate: bfloat16 [16, 2048, 1024], P('fs', None, 'tp')
- sample_up: bfloat16 [16, 2048, 1024], P('fs', None, 'tp')
- sample_down: bfloat16 [16, 2048, 1024], P('fs', None, 'tp')
- common_gate: bfloat16 [2048, 1024], P(None, 'tp')
- common_up: bfloat16 [2048, 1024], P(None, 'tp')
- common_down: bfloat16 [2048, 1024], P(None, 'tp')
Inputs may be any that keep to these rules, and one draw needn't show every extreme that they name: `routes`: each row names 6 different experts. In each aligned block of 256 rows (the rows of one index of fs) no expert is named by more than 160 rows, a bound that some expert reaches in some blocks.
All inputs are finite; a program needn't handle non-finite values.
Results may differ from a plain program's by a relative error of at most 0.015.
Values may be sent and summed in bfloat16 or wider, within the bound.
A program may use at most 128 MiB of HBM per device.

v0:
```python
import jax
import jax.numpy as jnp
from jax import lax
from jax.sharding import PartitionSpec as P

EPSILON = 1e-06


def normalize(tokens):
    values = tokens.astype(jnp.float32)
    scale = lax.rsqrt(jnp.mean(values * values, axis=-1, keepdims=True) + EPSILON)
    return (values * scale).astype(jnp.bfloat16)


def body(
    tokens,
    routes,
    route_weights,
    norm_gain,
    expert_gate,
    expert_up,
    expert_down,
    shared_gate,
    shared_up,
    shared_down,
):
    tp_count = lax.axis_size("tp")
    tp_index = lax.axis_index("tp")
    fs_count = lax.axis_size("fs")
    tok_rows, width = tokens.shape
    experts = expert_gate.shape[0]
    share = tok_rows // tp_count
    own_experts = experts // fs_count
    normed = normalize(tokens)
    own_normed = lax.dynamic_slice_in_dim(normed, tp_index * share, share, 0)
    own_routes = lax.dynamic_slice_in_dim(routes, tp_index * share, share, 0)
    own_weights = lax.dynamic_slice_in_dim(route_weights, tp_index * share, share, 0)
    member = own_routes[None, :, :] == jnp.arange(experts, dtype=jnp.int32)[:, None, None]
    dense = jnp.sum(jnp.where(member, own_weights[None, :, :], 0.0), axis=2)
    gathered = lax.all_gather(own_normed, "fs", axis=0, tiled=True)
    dense_all = lax.all_gather(dense, "fs", axis=0, tiled=False)
    gain_rows = norm_gain[None, :, None]
    rounded = (
        (expert_gate * gain_rows).astype(jnp.bfloat16),
        (expert_up * gain_rows).astype(jnp.bfloat16),
        expert_down.astype(jnp.bfloat16),
    )
    sample_gate, sample_up, sample_down = (
        lax.all_to_all(rounded[0], "fs", split_axis=0, concat_axis=1, tiled=True),
        lax.all_to_all(rounded[1], "fs", split_axis=0, concat_axis=1, tiled=True),
        lax.all_to_all(rounded[2], "fs", split_axis=0, concat_axis=1, tiled=True),
    )
    common_gate, common_up, common_down = (
        lax.all_gather(
            (shared_gate * norm_gain[:, None]).astype(jnp.bfloat16), "fs", axis=0, tiled=True
        ),
        lax.all_gather(
            (shared_up * norm_gain[:, None]).astype(jnp.bfloat16), "fs", axis=0, tiled=True
        ),
        lax.all_gather(shared_down.astype(jnp.bfloat16), "fs", axis=0, tiled=True),
    )
    shared_gate_act = jnp.dot(normed, common_gate, preferred_element_type=jnp.float32)
    shared_up_act = jnp.dot(normed, common_up, preferred_element_type=jnp.float32)
    shared_hidden = (jax.nn.silu(shared_gate_act) * shared_up_act).astype(jnp.bfloat16)
    shared_part = jnp.einsum(
        "th,dh->td", shared_hidden, common_down, preferred_element_type=jnp.float32
    ).astype(jnp.bfloat16)
    shared_parts = lax.all_to_all(
        shared_part.reshape(tok_rows, tp_count, width // tp_count).transpose(1, 0, 2),
        "tp",
        split_axis=0,
        concat_axis=0,
        tiled=True,
    )
    shared_sum = jnp.sum(shared_parts.astype(jnp.float32), axis=0)
    scale_all = lax.dynamic_slice_in_dim(
        dense_all, lax.axis_index("fs") * own_experts, own_experts, 1
    )
    total = None
    for expert in range(own_experts):
        scale = scale_all[:, expert, :].reshape(-1)[:, None]
        for shift in range(tp_count):
            gate_w, up_w, down_w = (sample_gate[expert], sample_up[expert], sample_down[expert])
            if shift:
                ring = [(i, (i + shift) % tp_count) for i in range(tp_count)]
                gate_w, up_w, down_w = (
                    lax.ppermute(gate_w, "tp", ring),
                    lax.ppermute(up_w, "tp", ring),
                    lax.ppermute(down_w, "tp", ring),
                )
            gate = jnp.dot(gathered, gate_w, preferred_element_type=jnp.float32)
            upward = jnp.dot(gathered, up_w, preferred_element_type=jnp.float32)
            hidden = (jax.nn.silu(gate) * upward * scale).astype(jnp.bfloat16)
            part = jnp.einsum("rf,df->rd", hidden, down_w, preferred_element_type=jnp.float32)
            total = part if total is None else total + part
    routed = lax.psum_scatter(total.astype(jnp.bfloat16), "fs", scatter_dimension=0, tiled=True)
    routed = lax.all_to_all(routed, "tp", split_axis=1, concat_axis=0, tiled=True)
    layer_output = (routed.astype(jnp.float32) + shared_sum).astype(jnp.bfloat16)
    return (layer_output, sample_gate, sample_up, sample_down, common_gate, common_up, common_down)


def solution(mesh):
    return jax.shard_map(
        body,
        mesh=mesh,
        in_specs=(
            P("fs", None),
            P("fs", None),
            P("fs", None),
            P("fs"),
            P(None, "fs", "tp"),
            P(None, "fs", "tp"),
            P(None, "fs", "tp"),
            P("fs", "tp"),
            P("fs", "tp"),
            P("fs", "tp"),
        ),
        out_specs=(
            P("fs", "tp"),
            P("fs", None, "tp"),
            P("fs", None, "tp"),
            P("fs", None, "tp"),
            P(None, "tp"),
            P(None, "tp"),
            P(None, "tp"),
        ),
        check_vma=False,
    )
```

profile of v0, /device:TPU:11, one launch (start us, length us, event | category | flops | bytes accessed | tf_op | source)
XLA Modules:
  0.0 607.8 jit_solution(15371878558450184911)
XLA Ops:
  7.2 0.0 copy-start
  7.2 0.0 copy-start.8
  7.2 0.0 all-gather.6.cloned.1.call-start
  7.2 1.5 fusion
  8.8 1.5 fusion.1
  10.2 0.8 constant_dynamic-slice_fusion.3
  11.1 0.0 all-gather.6.cloned.1.call-update
  11.1 0.0 copy-done.8
  11.1 6.8 %multiply_convert_fusion.2 = (bf16[16,128,512]{2,1,0:T(8,128)(2,1)}, bf16[16,128,512]{2,1,0:T(8,128)(2,1)}) fusion(f32[16,128,512]{2,1,0:T(8,128)} %param.15, f32[128]{0:T(128)S(1)} %copy-done.8, f32[16,128,512]{2,1,0:T(8,128)} %param.14), kind=kLoop, calls=%fused_computation.3 | loop fusion | flops 4194304 | bytes 12583424 | tf_op jit(solution)/shard_map/convert_element_type | solution.py:45
  17.9 6.8 %all-to-all-start = ((bf16[16,128,512]{2,1,0:T(8,128)(2,1)}), bf16[16,128,512]{2,1,0:T(8,128)(2,1)S(1)}, u32[]{:S(2)}, u32[]{:S(2)}) async-start(bf16[16,128,512]{2,1,0:T(8,128)(2,1)} %get-tuple-element.8), calls=%async_computation | async-start | bytes 4194304 | tf_op jit(solution)/shard_map/all_to_all | solution.py:49
  24.7 0.0 all-gather.8.cloned.1.call-start
  24.7 0.0 copy-done.6
  24.7 1.8 multiply_convert_fusion.6
  26.5 0.0 all-gather.8.cloned.1.call-update
  26.5 74.4 %all-to-all-done = bf16[16,128,512]{2,1,0:T(8,128)(2,1)S(1)} async-done(((bf16[16,128,512]{2,1,0:T(8,128)(2,1)}), bf16[16,128,512]{2,1,0:T(8,128)(2,1)S(1)}, u32[]{:S(2)}, u32[]{:S(2)}) %all-to-all-start) | async-done | bytes 2097184 | tf_op jit(solution)/shard_map/all_to_all | solution.py:49
  101.0 6.9 %all-to-all-start.1 = ((bf16[16,128,512]{2,1,0:T(8,128)(2,1)}), bf16[16,128,512]{2,1,0:T(8,128)(2,1)}, u32[]{:S(2)}, u32[]{:S(2)}) async-start(bf16[16,128,512]{2,1,0:T(8,128)(2,1)} %get-tuple-element.7), calls=%async_computation.1 | async-start | bytes 4194304 | tf_op jit(solution)/shard_map/all_to_all | solution.py:50
  107.8 0.0 all-gather.10.cloned.1.call-start
  107.9 0.7 all-gather.10.cloned.1.call-update
  108.6 0.0 copy-start.5
  108.6 0.0 copy-start.7
  108.6 3.9 convert_element_type.59
  112.5 81.0 %all-to-all-done.1 = bf16[16,128,512]{2,1,0:T(8,128)(2,1)} async-done(((bf16[16,128,512]{2,1,0:T(8,128)(2,1)}), bf16[16,128,512]{2,1,0:T(8,128)(2,1)}, u32[]{:S(2)}, u32[]{:S(2)}) %all-to-all-start.1) | async-done | bytes 2097184 | tf_op jit(solution)/shard_map/all_to_all | solution.py:50
  193.5 9.3 %all-to-all-start.2 = ((bf16[16,128,512]{2,1,0:T(8,128)(2,1)}), bf16[16,128,512]{2,1,0:T(8,128)(2,1)}, u32[]{:S(2)}, u32[]{:S(2)}) async-start(bf16[16,128,512]{2,1,0:T(8,128)(2,1)} %convert_element_type.59), calls=%async_computation.2 | async-start | bytes 4194304 | tf_op jit(solution)/shard_map/all_to_all | solution.py:51
  202.8 0.0 all-gather.12.cloned.1.call-start
  202.8 4.0 collective-permute-start
  206.8 0.0 copy-done.5
  206.9 0.7 convert_element_type.68
  207.5 0.0 all-gather.12.cloned.1.call-update
  207.5 0.0 reduce-scatter.2.cloned.1.call-start
  207.6 0.0 copy-done
  207.6 0.0 copy-done.7
  207.7 68.8 %all-gather = f32[256,128]{1,0:T(8,128)S(1)} all-gather(f32[16,128]{1,0:T(8,128)S(1)} %select_reduce_fusion), channel_id=2, replica_groups=mesh['fs'=16,'tp'=2] {'fs'}, dimensions={0}, use_global_device_ids=true | all-gather | bytes 139264 | tf_op jit(solution)/shard_map/all_gather | solution.py:41
  276.5 8.9 %collective-permute-start.1 = (bf16[2048,512]{1,0:T(8,128)(2,1)}, bf16[2048,512]{1,0:T(8,128)(2,1)}, u32[]{:S(2)}, u32[]{:S(2)}) collective-permute-start(bf16[2048,512]{1,0:T(8,128)(2,1)} %bitcast.1), channel_id=1, source_target_pairs={{0,1},{1,0},{2,3},{3,2},{4,5},{5,4},{6,7},{7,6},{8,9},{9,8},{10,11... | collective-permute-start | bytes 6291464 | tf_op jit(solution)/shard_map/ppermute | solution.py:88
  285.4 0.0 all-to-all-done.2
  285.4 0.1 collective-permute-start.2
  285.5 9.8 %fusion.16 = f32[2048,512]{1,0:T(8,128)} fusion(bf16[2048,2048]{1,0:T(8,128)(2,1)} %all-gather.6.cloned.1.call-done, bf16[2048,512]{1,0:T(8,128)(2,1)S(1)} %bitcast.41), kind=kOutput, calls=%fused_computation.38 | convolution fusion | flops 4294967296 | bytes 14680064 | tf_op jit(solution)/shard_map/dot_general | solution.py:91
  295.3 0.0 collective-permute-done
  295.3 0.0 copy-done.9
  295.3 7.6 %fusion.17 = f32[2048,512]{1,0:T(8,128)} fusion(bf16[2048,2048]{1,0:T(8,128)(2,1)S(1)} %copy-done.9, bf16[2048,512]{1,0:T(8,128)(2,1)} %collective-permute-done), kind=kOutput, calls=%fused_computation.39 | convolution fusion | flops 4294967296 | bytes 14680064 | tf_op jit(solution)/shard_map/dot_general | solution.py:91
  302.9 0.0 collective-permute-done.1
  302.9 7.6 %fusion.18 = f32[2048,512]{1,0:T(8,128)} fusion(bf16[2048,2048]{1,0:T(8,128)(2,1)S(1)} %copy-done.9, bf16[2048,512]{1,0:T(8,128)(2,1)} %collective-permute-done.1), kind=kOutput, calls=%fused_computation.40 | convolution fusion | flops 4294967296 | bytes 14680064 | tf_op jit(solution)/shard_map/dot_general | solution.py:92
  310.5 16.6 %fusion.6 = f32[2048,2048]{1,0:T(8,128)} fusion(bf16[2048,512]{1,0:T(8,128)(2,1)} %bitcast.4, f32[2048,512]{1,0:T(8,128)} %fusion.16, bf16[2048,2048]{1,0:T(8,128)(2,1)} %all-gather.6.cloned.1.call-done, bf16[2048,512]{1,0:T(8,128)(2,1)} %bitcast.1, f32[2048]{0:T(1024)S(1)} %bitcast.48), kind=kOutput, calls=%fused_computation.18 | convolution fusion | flops 8597274624 | bytes 33562624 | tf_op jit(solution)/shard_map/rf,df->rd/dot_general | solution.py:94
  327.0 0.0 collective-permute-done.2
  327.0 13.6 %add_convert_fusion = bf16[2048,2048]{1,0:T(8,128)(2,1)} fusion(f32[2048,2048]{1,0:T(8,128)} %fusion.6, bf16[2048,512]{1,0:T(8,128)(2,1)} %collective-permute-done.2, f32[2048,512]{1,0:T(8,128)} %fusion.18, f32[2048,512]{1,0:T(8,128)} %fusion.17, f32[2048]{0:T(1024)S(1)} %bitcast.49), kind=kOutput, calls=%fused_computation | convolution fusion | flops 4310695936 | bytes 35659776 | tf_op jit(solution)/shard_map/rf,df->rd/dot_general | solution.py:94
  340.6 0.0 reduce-scatter.2.cloned.1.call-update
  340.6 0.0 all-gather.8.cloned.1.call-done
  340.7 3.1 fusion.19
  343.8 55.0 %all-gather.12.cloned.1.call-done = bf16[2048,512]{1,0:T(8,128)(2,1)} async-done(((bf16[128,512]{1,0:T(8,128)(2,1)}), bf16[2048,512]{1,0:T(8,128)(2,1)}) %all-gather.12.cloned.1.call-update) | async-done | bytes 2097168 | tf_op jit(solution)/shard_map/all_gather | solution.py:60
  398.8 4.7 convolution_convert_fusion
  403.5 2.3 copy.30
  405.7 5.2 all-to-all-start.4
  410.9 1.7 all-to-all-done.4
  412.7 1.2 convert_reduce_fusion
  413.9 167.8 %reduce-scatter.2.cloned.1.call-done = bf16[128,2048]{1,0:T(8,128)(2,1)} async-done(((bf16[2048,2048]{1,0:T(8,128)(2,1)}), bf16[128,2048]{1,0:T(8,128)(2,1)}) %reduce-scatter.2.cloned.1.call-update) | async-done | bytes 524304 | tf_op jit(solution)/shard_map/reduce_scatter | solution.py:96
  581.7 1.1 copy.31
  582.8 4.7 all_to_all.54
  587.4 2.2 fusion.5
  589.6 1.3 copy.38
  590.9 3.2 copy.39
  594.1 3.2 copy.40
  597.3 1.3 copy.41
  598.7 1.3 copy.42
  600.0 1.3 copy.43
  601.3 0.0 copy-done.1
  (16 shorter events, 0.1 us)
Async XLA Ops:
  7.2 200.4 %copy-start = (f32[256,6]{0,1:T(8,128)S(1)}, f32[256,6]{0,1:T(8,128)}, u32[]{:S(2)}) copy-start(f32[256,6]{0,1:T(8,128)} %param.12) | copy-start | bytes 18436
  7.2 3.9 copy-start.8
  7.2 278.3 %all-gather.6.cloned.1.call-start = ((), (), s32[]{:S(2)}) async-start(), calls=%async_computation.6 | async-start | bytes 8912896 | tf_op jit(solution)/shard_map/all_gather | solution.py:40
  17.9 6.8 %copy-start.6 = (f32[128,512]{1,0:T(8,128)S(1)}, f32[128,512]{1,0:T(8,128)}, u32[]{:S(2)}) copy-start(f32[128,512]{1,0:T(8,128)} %param.17) | copy-start | bytes 786436
  17.9 83.0 %all-to-all-start = ((bf16[16,128,512]{2,1,0:T(8,128)(2,1)}), bf16[16,128,512]{2,1,0:T(8,128)(2,1)S(1)}, u32[]{:S(2)}, u32[]{:S(2)}) async-start(bf16[16,128,512]{2,1,0:T(8,128)(2,1)} %get-tuple-element.8), calls=%async_computation | async-start | bytes 4194304 | tf_op jit(solution)/shard_map/all_to_all | solution.py:49
  24.7 316.0 %all-gather.8.cloned.1.call-start = ((), (), s32[]{:S(2)}) async-start(), calls=%async_computation.8 | async-start | bytes 2228224 | tf_op jit(solution)/shard_map/all_gather | solution.py:54
  101.0 92.5 %all-to-all-start.1 = ((bf16[16,128,512]{2,1,0:T(8,128)(2,1)}), bf16[16,128,512]{2,1,0:T(8,128)(2,1)}, u32[]{:S(2)}, u32[]{:S(2)}) async-start(bf16[16,128,512]{2,1,0:T(8,128)(2,1)} %get-tuple-element.7), calls=%async_computation.1 | async-start | bytes 4194304 | tf_op jit(solution)/shard_map/all_to_all | solution.py:50
  107.8 235.9 %all-gather.10.cloned.1.call-start = ((), (), s32[]{:S(2)}) async-start(), calls=%async_computation.9 | async-start | bytes 2228224 | tf_op jit(solution)/shard_map/all_gather | solution.py:57
  108.6 98.3 %copy-start.5 = (f32[128,512]{1,0:T(8,128)S(1)}, f32[128,512]{1,0:T(8,128)}, u32[]{:S(2)}) copy-start(f32[128,512]{1,0:T(8,128)} %param.19) | copy-start | bytes 786436
  108.6 99.1 %copy-start.7 = (s32[256,6]{0,1:T(8,128)S(1)}, s32[256,6]{0,1:T(8,128)}, u32[]{:S(2)}) copy-start(s32[256,6]{0,1:T(8,128)} %param.11) | copy-start | bytes 18436
  193.5 91.9 %all-to-all-start.2 = ((bf16[16,128,512]{2,1,0:T(8,128)(2,1)}), bf16[16,128,512]{2,1,0:T(8,128)(2,1)}, u32[]{:S(2)}, u32[]{:S(2)}) async-start(bf16[16,128,512]{2,1,0:T(8,128)(2,1)} %convert_element_type.59), calls=%async_computation.2 | async-start | bytes 4194304 | tf_op jit(solution)/shard_map/all_to_all | solution.py:51
  202.8 196.0 %all-gather.12.cloned.1.call-start = ((), (), s32[]{:S(2)}) async-start(), calls=%async_computation.10 | async-start | bytes 2228224 | tf_op jit(solution)/shard_map/all_gather | solution.py:60
  202.8 92.5 %collective-permute-start = (bf16[2048,512]{1,0:T(8,128)(2,1)S(1)}, bf16[2048,512]{1,0:T(8,128)(2,1)}, u32[]{:S(2)}, u32[]{:S(2)}) collective-permute-start(bf16[2048,512]{1,0:T(8,128)(2,1)S(1)} %bitcast.40), channel_id=1, source_target_pairs={{0,1},{1,0},{2,3},{3,2},{4,5},{5,4},{6,7},{7,6},{8,9},{9,8},{10,11... | collective-permute-start | bytes 6291464 | tf_op jit(solution)/shard_map/ppermute | solution.py:87
  207.5 374.1 %reduce-scatter.2.cloned.1.call-start = ((), (), s32[]{:S(2)}) async-start(), calls=%async_computation.7 | async-start | bytes 8912896 | tf_op jit(solution)/shard_map/reduce_scatter | solution.py:96
  276.5 26.4 %collective-permute-start.1 = (bf16[2048,512]{1,0:T(8,128)(2,1)}, bf16[2048,512]{1,0:T(8,128)(2,1)}, u32[]{:S(2)}, u32[]{:S(2)}) collective-permute-start(bf16[2048,512]{1,0:T(8,128)(2,1)} %bitcast.1), channel_id=1, source_target_pairs={{0,1},{1,0},{2,3},{3,2},{4,5},{5,4},{6,7},{7,6},{8,9},{9,8},{10,11... | collective-permute-start | bytes 6291464 | tf_op jit(solution)/shard_map/ppermute | solution.py:88
  285.4 41.6 %collective-permute-start.2 = (bf16[2048,512]{1,0:T(8,128)(2,1)}, bf16[2048,512]{1,0:T(8,128)(2,1)}, u32[]{:S(2)}, u32[]{:S(2)}) collective-permute-start(bf16[2048,512]{1,0:T(8,128)(2,1)} %bitcast.4), channel_id=1, source_target_pairs={{0,1},{1,0},{2,3},{3,2},{4,5},{5,4},{6,7},{7,6},{8,9},{9,8},{10,11... | collective-permute-start | bytes 6291464 | tf_op jit(solution)/shard_map/ppermute | solution.py:89
  285.5 9.8 %copy-start.9 = (bf16[2048,2048]{1,0:T(8,128)(2,1)S(1)}, bf16[2048,2048]{1,0:T(8,128)(2,1)}, u32[]{:S(2)}) copy-start(bf16[2048,2048]{1,0:T(8,128)(2,1)} %all-gather.6.cloned.1.call-done) | copy-start | bytes 25165828
  405.7 6.9 %all-to-all-start.4 = ((bf16[2,256,1024]{2,1,0:T(8,128)(2,1)}), bf16[2,256,1024]{2,1,0:T(8,128)(2,1)S(1)}, u32[]{:S(2)}, u32[]{:S(2)}) async-start(bf16[2,256,1024]{2,1,0:T(8,128)(2,1)} %bitcast.43), calls=%async_computation.5 | async-start | bytes 2097152 | tf_op jit(solution)/shard_map/all_to_all | solution.py:68
  590.9 6.4 %copy-start.2 = (bf16[2048,512]{1,0:T(8,128)(2,1)S(1)}, bf16[2048,512]{1,0:T(8,128)(2,1)}, u32[]{:S(2)}) copy-start(bf16[2048,512]{1,0:T(8,128)(2,1)} %all-gather.8.cloned.1.call-done) | copy-start | bytes 6291460
  594.1 4.5 copy-start.3
  597.3 2.6 copy-start.4
  597.3 4.0 copy-start.1
Sparse Core Ops, SparseCore 0:
  11.3 187.2 all-gather.5
  202.0 71.4 all-gather.7
  276.8 59.5 all-gather.9
  339.6 59.1 all-gather.11
  400.9 180.7 reduce-scatter.1
where the time goes:
time: 609 us; the launch traced here: 608 us
  waiting for transfers between devices  381 us (63%)
  blocking collectives  73.5 us (12%)
  matrix products  62.9 us (10%)
  starting transfers between devices  41.3 us (7%)
  other arithmetic  19.5 us (3%)
  local copies, waits for them, and re-layouts  15.9 us (3%)
  between operations  13.9 us (2%)
    reduce_scatter x1, waiting for transfers between devices, body(): lax.psum_scatter(total.astype(jnp.bfloat16), 'fs', scatter_dimension=0, t...  168 us
    all_to_all x1, waiting for transfers between devices, body(): lax.all_to_all(rounded[1], 'fs', split_axis=0, concat_axis=1, tiled=True)  81 us
    all_to_all x1, waiting for transfers between devices, body(): lax.all_to_all(rounded[0], 'fs', split_axis=0, concat_axis=1, tiled=True)  74.4 us
    all_gather x1, blocking collectives, body(): dense_all = lax.all_gather(dense, 'fs', axis=0, tiled=False)  68.8 us
    all_gather x1, waiting for transfers between devices, body(): lax.all_gather(shared_down.astype(jnp.bfloat16), 'fs', axis=0, tiled=True)  55 us
    dot_general x2, matrix products, body(): jnp.einsum('rf,df->rd', hidden, down_w, preferred_element_type=jnp.float32)  30.1 us
    dot_general x2, matrix products, body(): gate = jnp.dot(gathered, gate_w, preferred_element_type=jnp.float32)  17.4 us
  transfers between devices with their start and end apart: 12, of which 5 were waited for; matrix products, arithmetic and copies ran while one was open for 13% of the time, Pallas kernels for 0%

commit v1 on v0

--- a/solution.py
+++ b/solution.py
@@ -4,6 +4,18 @@
 from jax.sharding import PartitionSpec as P
 
 EPSILON = 1e-06
+
+
+def doubled_up(shard, axis, dim):
+    ways, here, step = (lax.axis_size(axis), lax.axis_index(axis), shard.shape[dim])
+    line, have = (shard, 1)
+    while have < ways:
+        line = jnp.concatenate(
+            [line, lax.ppermute(line, axis, [(d, (d - have) % ways) for d in range(ways)])],
+            axis=dim,
+        )
+        have = 2 * have
+    return jnp.roll(line, here * step, axis=dim)
 
 
 def normalize(tokens):
@@ -57,7 +69,7 @@
         lax.all_gather(
             (shared_up * norm_gain[:, None]).astype(jnp.bfloat16), "fs", axis=0, tiled=True
         ),
-        lax.all_gather(shared_down.astype(jnp.bfloat16), "fs", axis=0, tiled=True),
+        doubled_up(shared_down.astype(jnp.bfloat16), "fs", 0),
     )
     shared_gate_act = jnp.dot(normed, common_gate, preferred_element_type=jnp.float32)
     shared_up_act = jnp.dot(normed, common_up, preferred_element_type=jnp.float32)

time: 609 us -> 551 us (0.905)
  waiting for transfers between devices: 381 us -> 233 us
  blocking collectives: 73.5 us -> 164 us
  local copies, waits for them, and re-layouts: 15.9 us -> 28.4 us
  starting transfers between devices: 41.3 us -> 29.3 us
    reduce_scatter x1, waiting for transfers between devices: 168 us -> 81.3 us  [body(): lax.psum_scatter(total.astype(jnp.bfloat16), 'fs', scatter_dimension=0, t...]
    all_to_all x0 -> x1, blocking collectives: none -> 85.9 us  [body(): lax.all_to_all(rounded[0], 'fs', split_axis=0, concat_axis=1, tiled=True)]
    all_to_all x1 -> x0, waiting for transfers between devices: 74.4 us -> none  [body(): lax.all_to_all(rounded[0], 'fs', split_axis=0, concat_axis=1, tiled=True)]
    ppermute x0 -> x4, waiting for transfers between devices: none -> 67.9 us  [doubled_up(): lax.ppermute(line, axis, [(d, (d - have) % ways) for d in range(ways)])]
    all_gather x1 -> x0, waiting for transfers between devices: 55 us -> none  [body(): lax.all_gather(shared_down.astype(jnp.bfloat16), 'fs', axis=0, tiled=True)]
    unnamed x26 -> x37, local copies, waits for them, and re-layouts: 11.7 us -> 18.7 us
    all_to_all x1 -> x0, starting transfers between devices: 6.77 us -> none  [body(): lax.all_to_all(rounded[0], 'fs', split_axis=0, concat_axis=1, tiled=True)]
  transfers between devices with their start and end apart: 12 -> 14, of which waited for: 5 -> 7; matrix products, arithmetic and copies ran while one was open for 13% -> 17% of each run, Pallas kernels for 0% -> 0%
where the time goes in v1:
time: 551 us
  waiting for transfers between devices  233 us (42%)
  blocking collectives  164 us (30%)
  matrix products  63.2 us (11%)
  starting transfers between devices  29.3 us (5%)
  local copies, waits for them, and re-layouts  28.4 us (5%)
  other arithmetic  18.9 us (3%)
  between operations  13.9 us (3%)
    all_to_all x1, blocking collectives, body(): lax.all_to_all(rounded[0], 'fs', split_axis=0, concat_axis=1, tiled=True)  85.9 us
    all_to_all x1, waiting for transfers between devices, body(): lax.all_to_all(rounded[1], 'fs', split_axis=0, concat_axis=1, tiled=True)  81.6 us
    reduce_scatter x1, waiting for transfers between devices, body(): lax.psum_scatter(total.astype(jnp.bfloat16), 'fs', scatter_dimension=0, t...  81.3 us
    all_gather x1, blocking collectives, body(): dense_all = lax.all_gather(dense, 'fs', axis=0, tiled=False)  72.2 us
    ppermute x4, waiting for transfers between devices, doubled_up(): lax.ppermute(line, axis, [(d, (d - have) % ways) for d in range(ways)])  67.9 us
    dot_general x2, matrix products, body(): jnp.einsum('rf,df->rd', hidden, down_w, preferred_element_type=jnp.float32)  30.2 us
    unnamed x37, local copies, waits for them, and re-layouts  18.7 us
    dot_general x2, matrix products, body(): gate = jnp.dot(gathered, gate_w, preferred_element_type=jnp.float32)  17.3 us
  transfers between devices with their start and end apart: 14, of which 7 were waited for; matrix products, arithmetic and copies ran while one was open for 17% of the time, Pallas kernels for 0%

profile of v1, /device:TPU:11, one launch (start us, length us, event | category | flops | bytes accessed | tf_op | source)
XLA Modules:
  0.0 550.7 jit_solution(6024421141377645320)
XLA Ops:
  7.2 0.0 copy-start
  7.2 0.0 all-gather.5.cloned.1.call-start
  7.2 1.5 fusion
  8.8 1.5 fusion.1
  10.2 0.9 constant_dynamic-slice_fusion.4
  11.2 0.0 all-gather.5.cloned.1.call-update
  11.2 6.1 %multiply_convert_fusion.2 = (bf16[16,128,512]{2,1,0:T(8,128)(2,1)}, bf16[16,128,512]{2,1,0:T(8,128)(2,1)S(1)}) fusion(f32[16,128,512]{2,1,0:T(8,128)} %param.15, f32[128]{0:T(128)S(1)} %copy-done.10, f32[16,128,512]{2,1,0:T(8,128)} %param.14), kind=kLoop, calls=%fused_computation.3 | loop fusion | flops 4194304 | bytes 12583424 | tf_op jit(solution)/shard_map/convert_element_type | solution.py:57
  17.3 85.9 %all_to_all.54 = bf16[16,128,512]{2,1,0:T(8,128)(2,1)S(1)} all-to-all(bf16[16,128,512]{2,1,0:T(8,128)(2,1)S(1)} %get-tuple-element.10), channel_id=1, replica_groups=mesh['fs'=16,'tp'=2] {'fs'}, dimensions={0} | all-to-all | bytes 4194304 | tf_op jit(solution)/shard_map/all_to_all | solution.py:61
  103.2 5.0 all-to-all-start.1
  108.2 0.0 all-gather.7.cloned.1.call-start
  108.3 0.8 multiply_convert_fusion.6
  109.1 0.0 all-gather.7.cloned.1.call-update
  109.1 3.9 convert_element_type.59
  113.0 81.6 %all-to-all-done.1 = bf16[16,128,512]{2,1,0:T(8,128)(2,1)} async-done(((bf16[16,128,512]{2,1,0:T(8,128)(2,1)}), bf16[16,128,512]{2,1,0:T(8,128)(2,1)}, u32[]{:S(2)}, u32[]{:S(2)}) %all-to-all-start.1) | async-done | bytes 2097184 | tf_op jit(solution)/shard_map/all_to_all | solution.py:62
  194.6 7.4 %all-to-all-start.2 = ((bf16[16,128,512]{2,1,0:T(8,128)(2,1)}), bf16[16,128,512]{2,1,0:T(8,128)(2,1)}, u32[]{:S(2)}, u32[]{:S(2)}) async-start(bf16[16,128,512]{2,1,0:T(8,128)(2,1)} %convert_element_type.59), calls=%async_computation.2 | async-start | bytes 4194304 | tf_op jit(solution)/shard_map/all_to_all | solution.py:63
  201.9 0.0 all-gather.9.cloned.1.call-start
  202.0 1.1 collective-permute-start
  203.1 0.0 all-gather.9.cloned.1.call-update
  203.1 0.0 reduce-scatter.2.cloned.1.call-start
  203.2 72.2 %all-gather = f32[256,128]{1,0:T(8,128)S(1)} all-gather(f32[16,128]{1,0:T(8,128)S(1)} %select_reduce_fusion), channel_id=2, replica_groups=mesh['fs'=16,'tp'=2] {'fs'}, dimensions={0}, use_global_device_ids=true | all-gather | bytes 139264 | tf_op jit(solution)/shard_map/all_gather | solution.py:53
  275.5 7.0 %collective-permute-start.1 = (bf16[2048,512]{1,0:T(8,128)(2,1)}, bf16[2048,512]{1,0:T(8,128)(2,1)}, u32[]{:S(2)}, u32[]{:S(2)}) collective-permute-start(bf16[2048,512]{1,0:T(8,128)(2,1)} %bitcast.1), channel_id=1, source_target_pairs={{0,1},{1,0},{2,3},{3,2},{4,5},{5,4},{6,7},{7,6},{8,9},{9,8},{10,11... | collective-permute-start | bytes 6291464 | tf_op jit(solution)/shard_map/ppermute | solution.py:100
  282.5 0.1 collective-permute-start.2
  282.6 9.7 %fusion.16 = f32[2048,512]{1,0:T(8,128)} fusion(bf16[2048,2048]{1,0:T(8,128)(2,1)} %all-gather.5.cloned.1.call-done, bf16[2048,512]{1,0:T(8,128)(2,1)S(1)} %bitcast.41), kind=kOutput, calls=%fused_computation.52 | convolution fusion | flops 4294967296 | bytes 14680064 | tf_op jit(solution)/shard_map/dot_general | solution.py:103
  292.3 7.6 %fusion.17 = f32[2048,512]{1,0:T(8,128)} fusion(bf16[2048,2048]{1,0:T(8,128)(2,1)S(1)} %copy-done.11, bf16[2048,512]{1,0:T(8,128)(2,1)} %collective-permute-done), kind=kOutput, calls=%fused_computation.53 | convolution fusion | flops 4294967296 | bytes 14680064 | tf_op jit(solution)/shard_map/dot_general | solution.py:103
  299.9 7.6 %fusion.18 = f32[2048,512]{1,0:T(8,128)} fusion(bf16[2048,2048]{1,0:T(8,128)(2,1)S(1)} %copy-done.11, bf16[2048,512]{1,0:T(8,128)(2,1)} %collective-permute-done.1), kind=kOutput, calls=%fused_computation.54 | convolution fusion | flops 4294967296 | bytes 14680064 | tf_op jit(solution)/shard_map/dot_general | solution.py:104
  307.5 16.6 %fusion.6 = f32[2048,2048]{1,0:T(8,128)} fusion(bf16[2048,512]{1,0:T(8,128)(2,1)} %bitcast.4, f32[2048,512]{1,0:T(8,128)} %fusion.16, bf16[2048,2048]{1,0:T(8,128)(2,1)} %all-gather.5.cloned.1.call-done, bf16[2048,512]{1,0:T(8,128)(2,1)} %bitcast.1, f32[2048]{0:T(1024)S(1)} %bitcast.48), kind=kOutput, calls=%fused_computation.19 | convolution fusion | flops 8597274624 | bytes 33562624 | tf_op jit(solution)/shard_map/rf,df->rd/dot_general | solution.py:106
  324.1 13.6 %add_convert_fusion = bf16[2048,2048]{1,0:T(8,128)(2,1)} fusion(f32[2048,2048]{1,0:T(8,128)} %fusion.6, bf16[2048,512]{1,0:T(8,128)(2,1)} %collective-permute-done.2, f32[2048,512]{1,0:T(8,128)} %fusion.18, f32[2048,512]{1,0:T(8,128)} %fusion.17, f32[2048]{0:T(1024)S(1)} %bitcast.49), kind=kOutput, calls=%fused_computation | convolution fusion | flops 4310695936 | bytes 35659776 | tf_op jit(solution)/shard_map/rf,df->rd/dot_general | solution.py:106
  337.6 0.0 reduce-scatter.2.cloned.1.call-update
  337.7 0.9 copy-done.6
  338.6 0.7 constant_dynamic-update-slice_fusion.9
  339.3 1.3 collective-permute-start.3
  340.5 4.3 collective-permute-done.3
  344.9 1.5 collective-permute-start.4
  346.4 9.9 %collective-permute-done.4 = bf16[256,512]{1,0:T(8,128)(2,1)S(1)} collective-permute-done((bf16[256,512]{1,0:T(8,128)(2,1)S(1)}, bf16[256,512]{1,0:T(8,128)(2,1)S(1)}, u32[]{:S(2)}, u32[]{:S(2)}) %collective-permute-start.4) | collective-permute-done | bytes 262176 | tf_op jit(solution)/shard_map/ppermute | solution.py:14
  356.3 0.3 collective-permute-start.5
  356.6 10.8 %collective-permute-done.5 = bf16[512,512]{1,0:T(8,128)(2,1)S(1)} collective-permute-done((bf16[512,512]{1,0:T(8,128)(2,1)S(1)}, bf16[512,512]{1,0:T(8,128)(2,1)S(1)}, u32[]{:S(2)}, u32[]{:S(2)}) %collective-permute-start.5) | collective-permute-done | bytes 524320 | tf_op jit(solution)/shard_map/ppermute | solution.py:14
  367.4 1.0 pad_maximum_fusion
  368.4 0.9 collective-permute-start.6
  369.3 0.7 constant_dynamic-update-slice_fusion.8
  370.0 0.7 constant_dynamic-update-slice_fusion.7
  370.7 0.8 constant_dynamic-update-slice_fusion.6
  371.5 43.0 %collective-permute-done.6 = bf16[1024,512]{1,0:T(8,128)(2,1)} collective-permute-done((bf16[1024,512]{1,0:T(8,128)(2,1)}, bf16[1024,512]{1,0:T(8,128)(2,1)}, u32[]{:S(2)}, u32[]{:S(2)}) %collective-permute-start.6) | collective-permute-done | bytes 1048608 | tf_op jit(solution)/shard_map/ppermute | solution.py:14
  414.5 2.3 constant_dynamic-update-slice_fusion.5
  416.7 0.7 constant_dynamic-update-slice_fusion.4
  417.4 0.7 constant_dynamic-update-slice_fusion.3
  418.1 0.7 constant_dynamic-update-slice_fusion.2
  418.8 0.8 constant_dynamic-update-slice_fusion.1
  419.6 2.3 constant_dynamic-update-slice_fusion
  421.9 3.1 constant_dynamic-slice_fusion
  425.0 3.4 fusion.19
  428.5 4.8 convolution_convert_fusion
  433.2 2.3 copy.30
  435.5 4.5 all-to-all-start.4
  440.1 1.7 all-to-all-done.4
  441.8 1.2 convert_reduce_fusion
  443.0 81.3 %reduce-scatter.2.cloned.1.call-done = bf16[128,2048]{1,0:T(8,128)(2,1)} async-done(((bf16[2048,2048]{1,0:T(8,128)(2,1)}), bf16[128,2048]{1,0:T(8,128)(2,1)}) %reduce-scatter.2.cloned.1.call-update) | async-done | bytes 524304 | tf_op jit(solution)/shard_map/reduce_scatter | solution.py:108
  524.2 1.1 copy.31
  525.3 6.3 %all_to_all.55 = bf16[128,2,1024]{2,0,1:T(8,128)(2,1)S(1)} all-to-all(bf16[128,2,1024]{2,0,1:T(8,128)(2,1)S(1)} %bitcast.44), channel_id=1, replica_groups=mesh['fs'=16,'tp'=2] {'tp'}, dimensions={1} | all-to-all | bytes 1048576 | tf_op jit(solution)/shard_map/all_to_all | solution.py:109
  531.6 2.2 fusion.5
  533.8 1.3 copy.46
  535.1 3.2 copy.47
  538.3 3.2 copy.48
  541.5 1.3 copy.49
  542.8 1.3 copy.50
  (36 shorter events, 0.2 us)
Async XLA Ops:
  7.2 196.0 %copy-start = (f32[256,6]{0,1:T(8,128)S(1)}, f32[256,6]{0,1:T(8,128)}, u32[]{:S(2)}) copy-start(f32[256,6]{0,1:T(8,128)} %param.12) | copy-start | bytes 18436
  7.2 4.0 copy-start.10
  7.2 275.4 %all-gather.5.cloned.1.call-start = ((), (), s32[]{:S(2)}) async-start(), calls=%async_computation.6 | async-start | bytes 8912896 | tf_op jit(solution)/shard_map/all_gather | solution.py:52
  10.2 7.1 %copy-start.2 = (bf16[256,2048]{1,0:T(8,128)(2,1)}, bf16[256,2048]{1,0:T(8,128)(2,1)S(1)}, u32[]{:S(2)}) copy-start(bf16[256,2048]{1,0:T(8,128)(2,1)S(1)} %fusion.1) | copy-start | bytes 3145732
  17.3 90.9 %copy-start.7 = (f32[128,512]{1,0:T(8,128)S(1)}, f32[128,512]{1,0:T(8,128)}, u32[]{:S(2)}) copy-start(f32[128,512]{1,0:T(8,128)} %param.17) | copy-start | bytes 786436
  17.3 90.9 %copy-start.8 = (f32[128,512]{1,0:T(8,128)S(1)}, f32[128,512]{1,0:T(8,128)}, u32[]{:S(2)}) copy-start(f32[128,512]{1,0:T(8,128)} %param.18) | copy-start | bytes 786436
  103.2 91.4 %all-to-all-start.1 = ((bf16[16,128,512]{2,1,0:T(8,128)(2,1)}), bf16[16,128,512]{2,1,0:T(8,128)(2,1)}, u32[]{:S(2)}, u32[]{:S(2)}) async-start(bf16[16,128,512]{2,1,0:T(8,128)(2,1)} %get-tuple-element.9), calls=%async_computation.1 | async-start | bytes 4194304 | tf_op jit(solution)/shard_map/all_to_all | solution.py:62
  108.2 316.8 %all-gather.7.cloned.1.call-start = ((), (), s32[]{:S(2)}) async-start(), calls=%async_computation.8 | async-start | bytes 2228224 | tf_op jit(solution)/shard_map/all_gather | solution.py:66
  109.1 94.1 %copy-start.9 = (s32[256,6]{0,1:T(8,128)S(1)}, s32[256,6]{0,1:T(8,128)}, u32[]{:S(2)}) copy-start(s32[256,6]{0,1:T(8,128)} %param.11) | copy-start | bytes 18436
  194.6 87.9 %all-to-all-start.2 = ((bf16[16,128,512]{2,1,0:T(8,128)(2,1)}), bf16[16,128,512]{2,1,0:T(8,128)(2,1)}, u32[]{:S(2)}, u32[]{:S(2)}) async-start(bf16[16,128,512]{2,1,0:T(8,128)(2,1)} %convert_element_type.59), calls=%async_computation.2 | async-start | bytes 4194304 | tf_op jit(solution)/shard_map/all_to_all | solution.py:63
  201.9 226.5 %all-gather.9.cloned.1.call-start = ((), (), s32[]{:S(2)}) async-start(), calls=%async_computation.9 | async-start | bytes 2228224 | tf_op jit(solution)/shard_map/all_gather | solution.py:69
  202.0 90.3 %collective-permute-start = (bf16[2048,512]{1,0:T(8,128)(2,1)S(1)}, bf16[2048,512]{1,0:T(8,128)(2,1)}, u32[]{:S(2)}, u32[]{:S(2)}) collective-permute-start(bf16[2048,512]{1,0:T(8,128)(2,1)S(1)} %bitcast.40), channel_id=1, source_target_pairs={{0,1},{1,0},{2,3},{3,2},{4,5},{5,4},{6,7},{7,6},{8,9},{9,8},{10,11... | collective-permute-start | bytes 6291464 | tf_op jit(solution)/shard_map/ppermute | solution.py:99
  203.1 321.1 %reduce-scatter.2.cloned.1.call-start = ((), (), s32[]{:S(2)}) async-start(), calls=%async_computation.7 | async-start | bytes 8912896 | tf_op jit(solution)/shard_map/reduce_scatter | solution.py:108
  275.5 24.4 %collective-permute-start.1 = (bf16[2048,512]{1,0:T(8,128)(2,1)}, bf16[2048,512]{1,0:T(8,128)(2,1)}, u32[]{:S(2)}, u32[]{:S(2)}) collective-permute-start(bf16[2048,512]{1,0:T(8,128)(2,1)} %bitcast.1), channel_id=1, source_target_pairs={{0,1},{1,0},{2,3},{3,2},{4,5},{5,4},{6,7},{7,6},{8,9},{9,8},{10,11... | collective-permute-start | bytes 6291464 | tf_op jit(solution)/shard_map/ppermute | solution.py:100
  282.5 41.6 %collective-permute-start.2 = (bf16[2048,512]{1,0:T(8,128)(2,1)}, bf16[2048,512]{1,0:T(8,128)(2,1)}, u32[]{:S(2)}, u32[]{:S(2)}) collective-permute-start(bf16[2048,512]{1,0:T(8,128)(2,1)} %bitcast.4), channel_id=1, source_target_pairs={{0,1},{1,0},{2,3},{3,2},{4,5},{5,4},{6,7},{7,6},{8,9},{9,8},{10,11... | collective-permute-start | bytes 6291464 | tf_op jit(solution)/shard_map/ppermute | solution.py:101
  282.6 9.7 %copy-start.11 = (bf16[2048,2048]{1,0:T(8,128)(2,1)S(1)}, bf16[2048,2048]{1,0:T(8,128)(2,1)}, u32[]{:S(2)}) copy-start(bf16[2048,2048]{1,0:T(8,128)(2,1)} %all-gather.5.cloned.1.call-done) | copy-start | bytes 25165828
  337.6 0.9 copy-start.6
  339.3 5.6 %collective-permute-start.3 = (bf16[128,512]{1,0:T(8,128)(2,1)S(1)}, bf16[128,512]{1,0:T(8,128)(2,1)S(1)}, u32[]{:S(2)}, u32[]{:S(2)}) collective-permute-start(bf16[128,512]{1,0:T(8,128)(2,1)S(1)} %get-tuple-element.8), channel_id=1, source_target_pairs={{0,30},{2,0},{4,2},{6,4},{8,6},{10,8},{12,10},{14,12},{16,14},{18,... | collective-permute-start | bytes 393224 | tf_op jit(solution)/shard_map/ppermute | solution.py:14
  344.9 11.4 %collective-permute-start.4 = (bf16[256,512]{1,0:T(8,128)(2,1)S(1)}, bf16[256,512]{1,0:T(8,128)(2,1)S(1)}, u32[]{:S(2)}, u32[]{:S(2)}) collective-permute-start(bf16[256,512]{1,0:T(8,128)(2,1)S(1)} %pad_maximum_fusion.2), channel_id=1, source_target_pairs={{0,28},{2,30},{4,0},{6,2},{8,4},{10,6},{12,8},{14,10},{16,12},{18,... | collective-permute-start | bytes 786440 | tf_op jit(solution)/shard_map/ppermute | solution.py:14
  356.3 11.1 %collective-permute-start.5 = (bf16[512,512]{1,0:T(8,128)(2,1)S(1)}, bf16[512,512]{1,0:T(8,128)(2,1)S(1)}, u32[]{:S(2)}, u32[]{:S(2)}) collective-permute-start(bf16[512,512]{1,0:T(8,128)(2,1)S(1)} %pad_maximum_fusion.1), channel_id=1, source_target_pairs={{0,24},{2,26},{4,28},{6,30},{8,0},{10,2},{12,4},{14,6},{16,8},{18,... | collective-permute-start | bytes 1572872 | tf_op jit(solution)/shard_map/ppermute | solution.py:14
  368.4 46.0 %collective-permute-start.6 = (bf16[1024,512]{1,0:T(8,128)(2,1)}, bf16[1024,512]{1,0:T(8,128)(2,1)}, u32[]{:S(2)}, u32[]{:S(2)}) collective-permute-start(bf16[1024,512]{1,0:T(8,128)(2,1)} %pad_maximum_fusion), channel_id=1, source_target_pairs={{0,16},{2,18},{4,20},{6,22},{8,24},{10,26},{12,28},{14,30},{16,0},... | collective-permute-start | bytes 3145736 | tf_op jit(solution)/shard_map/ppermute | solution.py:14
  421.9 6.6 %copy-start.3 = (bf16[256,2048]{1,0:T(8,128)(2,1)S(1)}, bf16[256,2048]{1,0:T(8,128)(2,1)}, u32[]{:S(2)}) copy-start(bf16[256,2048]{1,0:T(8,128)(2,1)} %copy-done.2) | copy-start | bytes 3145732
  435.5 6.3 %all-to-all-start.4 = ((bf16[2,256,1024]{2,1,0:T(8,128)(2,1)}), bf16[2,256,1024]{2,1,0:T(8,128)(2,1)S(1)}, u32[]{:S(2)}, u32[]{:S(2)}) async-start(bf16[2,256,1024]{2,1,0:T(8,128)(2,1)} %bitcast.43), calls=%async_computation.5 | async-start | bytes 2097152 | tf_op jit(solution)/shard_map/all_to_all | solution.py:80
  535.1 6.4 %copy-start.4 = (bf16[2048,512]{1,0:T(8,128)(2,1)S(1)}, bf16[2048,512]{1,0:T(8,128)(2,1)}, u32[]{:S(2)}) copy-start(bf16[2048,512]{1,0:T(8,128)(2,1)} %all-gather.7.cloned.1.call-done) | copy-start | bytes 6291460
  538.3 4.5 copy-start.5
  538.3 5.8 %copy-start.1 = (f32[256,6]{0,1:T(8,128)S(1)}, f32[256,6]{0,1:T(8,128)}, u32[]{:S(2)}) copy-start(f32[256,6]{0,1:T(8,128)} %param.12) | copy-start | bytes 18436
Sparse Core Ops, SparseCore 0:
  11.3 181.1 all-gather.4
  195.9 80.8 all-gather.6
  280.2 59.4 all-gather.8
  341.9 182.3 reduce-scatter.1
